TPU v7x, 128 devices: a whole 4x4x4 slice. The times are simulated.
128 devices in a mesh: tp: 16 (over z, x), dp: 8 (over y, core).
Axes of the slice: x: 4, y: 4, z: 4, core: 2. Of those that a mesh axis runs over, the one named last changes fastest.
Arguments:
- tokens: bfloat16 [224, 4096], P('tp', 'dp'), may hold values from -6 to 6
- w_query: bfloat16 [2, 4096, 4096], P(None, 'dp', 'tp'), may hold values from -0.09375 to 0.09375
- w_key: bfloat16 [2, 4096, 4096], P(None, 'dp', 'tp'), may hold values from -0.09375 to 0.09375
- w_value: bfloat16 [2, 4096, 4096], P(None, 'dp', 'tp'), may hold values from -0.09375 to 0.09375
- w_outgate: bfloat16 [2, 4096, 4096], P(None, 'dp', 'tp'), may hold values from -0.09375 to 0.09375
- w_ingate: bfloat16 [2, 4096, 32], P(None, 'dp'), may hold values from -0.09375 to 0.09375
- w_forget: bfloat16 [2, 4096, 32], P(None, 'dp'), may hold values from -0.09375 to 0.09375
- forget_bias: float32 [2, 32], P(None, 'tp'), may hold values from -2 to 3
- head_gain: float32 [2, 32, 128], P(None, 'tp'), may hold values from 0.1 to 1.9
- w_proj: bfloat16 [2, 4096, 4096], P(None, 'tp', 'dp'), may hold values from -0.09375 to 0.09375
- mem_matrix: float32 [2, 224, 32, 128, 128], P(None, 'dp', 'tp'), may hold values from -0.8 to 0.8
- mem_norm: float32 [2, 224, 32, 128], P(None, 'dp', 'tp'), may hold values from -1.2 to 1.2
- mem_max: float32 [2, 224, 32], P(None, 'dp', 'tp'), may hold values from -4 to 4
Outputs:
- result: bfloat16 [224, 4096], P('tp', 'dp')
- new_matrix: float32 [2, 224, 32, 128, 128], P(None, 'dp', 'tp')
- new_norm: float32 [2, 224, 32, 128], P(None, 'dp', 'tp')
- new_max: float32 [2, 224, 32], P(None, 'dp', 'tp')
All inputs are finite; a program needn't handle non-finite values.
Results may differ from a plain program's by a relative error of at most 0.017.
Values may be sent and summed in bfloat16 or wider, within the bound.
A program may use at most 128 MiB of HBM per device.

v0:
```python
import jax
import jax.numpy as jnp
from jax import lax
from jax.sharding import PartitionSpec as P

HEAD = 128


norm_eps = 1e-06
head_eps = 1e-05


def from_everyone(value, axis):
    count = lax.axis_size(axis)
    return lax.all_to_all(
        jnp.broadcast_to(value[None], (count, *value.shape)), axis, 0, 0, tiled=True
    )


def taken_together(value, axis):
    everything = from_everyone(value, axis)
    return jnp.sum(everything, axis=0)


def in_blocks(value, dim, count):
    before, after = (value.shape[:dim], value.shape[dim + 1 :])
    return jnp.moveaxis(value.reshape(*before, count, -1, *after), dim, 0)


def sum_at_owner(value, axis, dim):
    count = lax.axis_size(axis)
    tiles = lax.all_to_all(in_blocks(value, dim, count), axis, 0, 0, tiled=True)
    return jnp.sum(tiles, axis=0)


def in_one_piece(arrays, axis, dim, along):
    ends, at = ([], 0)
    for a in arrays[:-1]:
        at += a.shape[along]
        ends.append(at)
    both = jnp.concatenate(arrays, axis=along)
    return tuple(jnp.split(sum_at_owner(both, axis, dim), ends, axis=along))


def in_order(tiles, dim):
    tiles = jnp.moveaxis(tiles, 0, dim)
    dims = tiles.shape
    return tiles.reshape(*dims[:dim], dims[dim] * dims[dim + 1], *dims[dim + 2 :])


def collect(value, axis, dim):
    tiles = from_everyone(value, axis)
    return in_order(tiles, dim)


def sum_at_owner_2(value, axis, dim):
    count = lax.axis_size(axis)
    tiles = lax.all_to_all(in_blocks(value, dim, count), axis, 0, 0, tiled=True)
    return jnp.sum(tiles.astype(jnp.float32), axis=0)


def cell_update(queries, key_vecs, values, log_in, log_forget, matrix, normvec, maxval):
    max_next = jnp.maximum(log_forget + maxval, log_in)
    decays = jnp.exp(log_forget + maxval - max_next)
    weight_in = jnp.exp(log_in - max_next)
    matrix_new = (
        decays[..., None, None] * matrix
        + weight_in[..., None, None] * key_vecs[..., :, None] * values[..., None, :]
    )
    norm_new = decays[..., None] * normvec + weight_in[..., None] * key_vecs
    numerator = jnp.einsum("bhd,bhde->bhe", queries, matrix_new, precision=lax.Precision.HIGHEST)
    denominator = jnp.maximum(jnp.abs(jnp.sum(queries * norm_new, axis=-1)), 1.0)
    return (numerator / denominator[..., None], matrix_new, norm_new, max_next)


def head_norm(readout, gain, outgate):
    average = jnp.mean(readout, axis=-1, keepdims=True)
    variance = jnp.mean(jnp.square(readout - average), axis=-1, keepdims=True)
    normed = (readout - average) * lax.rsqrt(variance + head_eps) * gain
    return normed * jax.nn.sigmoid(outgate)


def mix_block(gathered, weights, states):
    w_query, w_key, w_value, w_outgate, w_ingate, w_forget, bias, gain, w_proj = weights
    matrix, normvec, maxval = states
    features = gathered.shape[1] * lax.axis_size("dp")
    squares = jnp.sum(jnp.square(gathered.astype(jnp.float32)), axis=1)
    heads_dev = bias.shape[0]
    head_start = lax.axis_index("tp") * heads_dev
    gate_in = lax.dynamic_slice_in_dim(w_ingate, head_start, heads_dev, 1)
    gate_forget = lax.dynamic_slice_in_dim(w_forget, head_start, heads_dev, 1)
    part_query = jnp.dot(gathered, w_query, preferred_element_type=jnp.float32)
    part_key = jnp.dot(gathered, w_key, preferred_element_type=jnp.float32)
    part_value = jnp.dot(gathered, w_value, preferred_element_type=jnp.float32)
    part_outgate = jnp.dot(gathered, w_outgate, preferred_element_type=jnp.float32)
    part_ingate = jnp.dot(gathered, gate_in, preferred_element_type=jnp.float32)
    part_forget = jnp.dot(gathered, gate_forget, preferred_element_type=jnp.float32)
    rows_dev = gathered.shape[0] // lax.axis_size("dp")
    totals = taken_together(squares, "dp")
    own_sum = lax.dynamic_slice_in_dim(totals, lax.axis_index("dp") * rows_dev, rows_dev, 0)
    sum_query, sum_key, sum_value, sum_outgate, sum_ingate, sum_forget = in_one_piece(
        (part_query, part_key, part_value, part_outgate, part_ingate, part_forget), "dp", 0, 1
    )
    inv_scale = lax.rsqrt(own_sum / features + norm_eps)[:, None]
    head_shape = (rows_dev, heads_dev, HEAD)
    queries = (sum_query * inv_scale).reshape(head_shape)
    key_vecs = (sum_key * inv_scale * HEAD ** (-0.5)).reshape(head_shape)
    values = (sum_value * inv_scale).reshape(head_shape)
    outgate = (sum_outgate * inv_scale).reshape(head_shape)
    log_in = sum_ingate * inv_scale
    log_forget = jax.nn.log_sigmoid(sum_forget * inv_scale + bias[None, :])
    readout, matrix_new, norm_new, max_next = cell_update(
        queries, key_vecs, values, log_in, log_forget, matrix, normvec, maxval
    )
    hidden = head_norm(readout, gain[None], outgate).reshape(rows_dev, -1).astype(jnp.bfloat16)
    out_partial = jnp.dot(collect(hidden, "dp", 0), w_proj, preferred_element_type=jnp.float32)
    return (out_partial, matrix_new, norm_new, max_next)


def on_device(
    tokens,
    w_query,
    w_key,
    w_value,
    w_outgate,
    w_ingate,
    w_forget,
    forget_bias,
    head_gain,
    w_proj,
    mem_matrix,
    mem_norm,
    mem_max,
):
    current = collect(tokens, "tp", 0)
    matrix_list, norm_list, max_list = ([], [], [])
    block_total = w_query.shape[0]
    result = current
    for block_id in range(block_total):
        weights = (
            w_query[block_id],
            w_key[block_id],
            w_value[block_id],
            w_outgate[block_id],
            w_ingate[block_id],
            w_forget[block_id],
            forget_bias[block_id],
            head_gain[block_id],
            w_proj[block_id],
        )
        out_partial, matrix_out, norm_out, max_out = mix_block(
            current, weights, (mem_matrix[block_id], mem_norm[block_id], mem_max[block_id])
        )
        matrix_list.append(matrix_out)
        norm_list.append(norm_out)
        max_list.append(max_out)
        if block_id + 1 < block_total:
            own_rows = sum_at_owner(out_partial, "tp", 0).astype(jnp.bfloat16)
            current = collect(own_rows, "tp", 0)
        else:
            result = sum_at_owner_2(out_partial.astype(jnp.bfloat16), "tp", 0).astype(jnp.bfloat16)
    return (result, jnp.stack(matrix_list), jnp.stack(norm_list), jnp.stack(max_list))


def solution(mesh):
    in_specs = (
        P("tp", "dp"),
        P(None, "dp", "tp"),
        P(None, "dp", "tp"),
        P(None, "dp", "tp"),
        P(None, "dp", "tp"),
        P(None, "dp", None),
        P(None, "dp", None),
        P(None, "tp"),
        P(None, "tp", None),
        P(None, "tp", "dp"),
        P(None, "dp", "tp", None, None),
        P(None, "dp", "tp", None),
        P(None, "dp", "tp"),
    )
    out_specs = (
        P("tp", "dp"),
        P(None, "dp", "tp", None, None),
        P(None, "dp", "tp", None),
        P(None, "dp", "tp"),
    )
    return jax.shard_map(
        on_device, mesh=mesh, in_specs=in_specs, out_specs=out_specs, check_vma=False
    )
```

profile of v0, /device:TPU:9, one launch (start us, length us, event | category | flops | bytes accessed | tf_op | source)
XLA Modules:
  0.0 162.4 jit_solution(14992166652110990135)
XLA Ops:
  0.6 1.5 broadcast_in_dim.16
  2.1 7.6 %all-to-all-start = ((bf16[16,14,512]{2,1,0:T(8,128)(2,1)}), bf16[16,14,512]{2,1,0:T(8,128)(2,1)S(1)}, u32[]{:S(2)}, u32[]{:S(2)}) async-start(bf16[16,14,512]{2,1,0:T(8,128)(2,1)} %broadcast_in_dim.16), calls=%async_computation | async-start | bytes 524288 | tf_op jit(solution)/shard_map/all_to_all | solution.py:15
  9.8 1.4 fusion.90
  11.2 1.4 fusion.89
  12.5 4.7 %all-to-all-done = bf16[16,14,512]{2,1,0:T(8,128)(2,1)S(1)} async-done(((bf16[16,14,512]{2,1,0:T(8,128)(2,1)}), bf16[16,14,512]{2,1,0:T(8,128)(2,1)S(1)}, u32[]{:S(2)}, u32[]{:S(2)}) %all-to-all-start) | async-done | bytes 229408 | tf_op jit(solution)/shard_map/all_to_all | solution.py:15
  18.1 6.6 %all-to-all-start.2 = ((f32[8,1,224]{2,1,0:T(1,128)}), f32[8,1,224]{2,1,0:T(1,128)S(1)}, u32[]{:S(2)}, u32[]{:S(2)}) async-start(f32[8,1,224]{2,1,0:T(1,128)} %broadcast_in_dim.18), calls=%async_computation.2 | async-start | bytes 16384 | tf_op jit(solution)/shard_map/all_to_all | solution.py:15
  24.8 1.2 fusion.27
  26.0 1.2 fusion.29
  27.2 1.2 fusion.31
  29.4 1.1 reshape.187
  30.5 4.8 %all-to-all-start.1 = ((f32[8,28,1028]{2,1,0:T(8,128)}), f32[8,28,1028]{2,1,0:T(8,128)S(1)}, u32[]{:S(2)}, u32[]{:S(2)}) async-start(f32[8,28,1028]{2,1,0:T(8,128)} %reshape.187), calls=%async_computation.1 | async-start | bytes 2359296 | tf_op jit(solution)/shard_map/all_to_all | solution.py:32
  36.7 13.9 %all-to-all-done.1 = f32[8,28,1028]{2,1,0:T(8,128)S(1)} async-done(((f32[8,28,1028]{2,1,0:T(8,128)}), f32[8,28,1028]{2,1,0:T(8,128)S(1)}, u32[]{:S(2)}, u32[]{:S(2)}) %all-to-all-start.1) | async-done | bytes 921120 | tf_op jit(solution)/shard_map/all_to_all | solution.py:32
  51.6 5.6 %fusion.4 = f32[28,2,1,128]{3,2,1,0:T(1,128)S(1)} fusion(f32[28,2,128,1]{2,3,1,0:T(1,128)S(1)} %bitcast.121, f32[2,28,2,128,128]{4,3,2,1,0:T(8,128)} %param.23, f32[28,2,128]{2,1,0:T(2,128)S(1)} %mul.321, f32[28,2,128]{2,1,0:T(2,128)S(1)} %get-tuple-element.13, f32[28,2]{1,0:T(8,128)S(1)} %get-tuple-element.14), kind=kOutput, calls=%fused_computation.6 | convolution fusion | flops 13762560 | bytes 3784928 | tf_op jit(solution)/shard_map/bhd,bhde->bhe/dot_general | solution.py:71
  57.9 8.6 %all_to_all.52 = bf16[8,28,256]{2,1,0:T(8,128)(2,1)S(1)} all-to-all(bf16[8,28,256]{2,1,0:T(8,128)(2,1)S(1)} %broadcast_in_dim.19), channel_id=1, replica_groups=mesh['tp'=16,'dp'=8] {'dp'}, dimensions={0} | all-to-all | bytes 229376 | tf_op jit(solution)/shard_map/all_to_all | solution.py:15
  66.7 13.1 %all_to_all.53 = f32[16,14,512]{2,1,0:T(8,128)S(1)} all-to-all(f32[16,14,512]{2,1,0:T(8,128)S(1)} %fusion.25), channel_id=1, replica_groups=mesh['tp'=16,'dp'=8] {'tp'}, dimensions={0} | all-to-all | bytes 917504 | tf_op jit(solution)/shard_map/all_to_all | solution.py:32
  79.9 10.5 %all_to_all.54 = bf16[16,14,512]{2,1,0:T(8,128)(2,1)S(1)} all-to-all(bf16[16,14,512]{2,1,0:T(8,128)(2,1)S(1)} %broadcast_in_dim.20), channel_id=1, replica_groups=mesh['tp'=16,'dp'=8] {'tp'}, dimensions={0} | all-to-all | bytes 458752 | tf_op jit(solution)/shard_map/all_to_all | solution.py:15
  92.3 7.4 %all-to-all-start.7 = ((f32[8,1,224]{2,1,0:T(1,128)}), f32[8,1,224]{2,1,0:T(1,128)S(1)}, u32[]{:S(2)}, u32[]{:S(2)}) async-start(f32[8,1,224]{2,1,0:T(1,128)} %broadcast_in_dim.22), calls=%async_computation.7 | async-start | bytes 16384 | tf_op jit(solution)/shard_map/all_to_all | solution.py:15
  99.7 0.9 fusion.71
  100.6 0.9 fusion.73
  101.8 1.1 reshape.190
  103.3 5.2 %all-to-all-start.6 = ((f32[8,28,1028]{2,1,0:T(8,128)}), f32[8,28,1028]{2,1,0:T(8,128)S(1)}, u32[]{:S(2)}, u32[]{:S(2)}) async-start(f32[8,28,1028]{2,1,0:T(8,128)} %reshape.190), calls=%async_computation.6 | async-start | bytes 2359296 | tf_op jit(solution)/shard_map/all_to_all | solution.py:32
  109.4 14.4 %all-to-all-done.6 = f32[8,28,1028]{2,1,0:T(8,128)S(1)} async-done(((f32[8,28,1028]{2,1,0:T(8,128)}), f32[8,28,1028]{2,1,0:T(8,128)S(1)}, u32[]{:S(2)}, u32[]{:S(2)}) %all-to-all-start.6) | async-done | bytes 921120 | tf_op jit(solution)/shard_map/all_to_all | solution.py:32
  126.5 7.5 %multiply_add_fusion.1 = (f32[1,28,2,128,128]{4,3,2,1,0:T(8,128)}, f32[1,28,2,128,128]{4,3,2,1,0:T(8,128)}) fusion(f32[2,28,2,128,128]{4,3,2,1,0:T(8,128)} %param.23, f32[28,2,128]{2,1,0:T(2,128)S(1)} %copy-done.11, f32[28,2,128]{2,1,0:T(2,128)S(1)} %copy-done.9, f32[28,2]{1,0:T(8,128)S(1)} %get-tuple-element.14, f32[28,2,128]{2,1,0:T(2,128)S(1)} %mul.347, ...), kind=kLoop, calls=%fused_computation.8 | loop fusion | flops 5505024 | bytes 14795200 | tf_op jit(solution)/shard_map/add | solution.py:67
  134.1 3.5 %fusion.1 = f32[28,2,1,128]{3,2,1,0:T(1,128)S(1)} fusion(f32[28,2,128,1]{2,3,1,0:T(1,128)S(1)} %bitcast.122, f32[2,28,2,128,128]{4,3,2,1,0:T(8,128)S(1)} %bitcast.116, f32[28,2,128]{2,1,0:T(2,128)S(1)} %mul.347, f32[28,2,128]{2,1,0:T(2,128)S(1)} %get-tuple-element.7, f32[28,2]{1,0:T(8,128)S(1)} %get-tuple-element.8), kind=kOutput, calls=%fused_computation.3 | convolution fusion | flops 13762560 | bytes 3801088 | tf_op jit(solution)/shard_map/bhd,bhde->bhe/dot_general | solution.py:71
  138.2 0.7 broadcast_in_dim.23
  138.9 5.3 %all-to-all-start.8 = ((bf16[8,28,256]{2,1,0:T(8,128)(2,1)}), bf16[8,28,256]{2,1,0:T(8,128)(2,1)S(1)}, u32[]{:S(2)}, u32[]{:S(2)}) async-start(bf16[8,28,256]{2,1,0:T(8,128)(2,1)} %broadcast_in_dim.23), calls=%async_computation.8 | async-start | bytes 262144 | tf_op jit(solution)/shard_map/all_to_all | solution.py:15
  145.6 2.8 %all-to-all-done.8 = bf16[8,28,256]{2,1,0:T(8,128)(2,1)S(1)} async-done(((bf16[8,28,256]{2,1,0:T(8,128)(2,1)}), bf16[8,28,256]{2,1,0:T(8,128)(2,1)S(1)}, u32[]{:S(2)}, u32[]{:S(2)}) %all-to-all-start.8) | async-done | bytes 114720 | tf_op jit(solution)/shard_map/all_to_all | solution.py:15
  148.4 1.2 convolution_convert_fusion
  149.6 0.8 reshape.193
  150.4 3.5 %all-to-all-start.9 = ((bf16[16,14,512]{2,1,0:T(8,128)(2,1)}), bf16[16,14,512]{2,1,0:T(8,128)(2,1)S(1)}, u32[]{:S(2)}, u32[]{:S(2)}) async-start(bf16[16,14,512]{2,1,0:T(8,128)(2,1)} %reshape.193), calls=%async_computation.9 | async-start | bytes 524288 | tf_op jit(solution)/shard_map/all_to_all | solution.py:58
  153.9 7.2 %pad_maximum_fusion = f32[2,28,2,128,128]{4,3,2,1,0:T(8,128)} fusion(f32[1,28,2,128,128]{4,3,2,1,0:T(8,128)} %get-tuple-element.17, f32[1,28,2,128,128]{4,3,2,1,0:T(8,128)} %get-tuple-element.16), kind=kLoop, calls=%fused_computation | loop fusion | flops 1835008 | bytes 14680064 | tf_op jit(solution)/shard_map/stack | solution.py:162
  161.1 0.7 all-to-all-done.9
  (125 shorter events, 13.5 us)
Async XLA Ops:
  0.6 27.7 %copy-start.4 = (bf16[2,512,256]{2,1,0:T(8,128)(2,1)S(1)}, bf16[2,512,256]{2,1,0:T(8,128)(2,1)}, u32[]{:S(2)}) copy-start(bf16[2,512,256]{2,1,0:T(8,128)(2,1)} %param.14) | copy-start | bytes 1572868
  2.1 15.1 %all-to-all-start = ((bf16[16,14,512]{2,1,0:T(8,128)(2,1)}), bf16[16,14,512]{2,1,0:T(8,128)(2,1)S(1)}, u32[]{:S(2)}, u32[]{:S(2)}) async-start(bf16[16,14,512]{2,1,0:T(8,128)(2,1)} %broadcast_in_dim.16), calls=%async_computation | async-start | bytes 524288 | tf_op jit(solution)/shard_map/all_to_all | solution.py:15
  18.1 12.3 %all-to-all-start.2 = ((f32[8,1,224]{2,1,0:T(1,128)}), f32[8,1,224]{2,1,0:T(1,128)S(1)}, u32[]{:S(2)}, u32[]{:S(2)}) async-start(f32[8,1,224]{2,1,0:T(1,128)} %broadcast_in_dim.18), calls=%async_computation.2 | async-start | bytes 16384 | tf_op jit(solution)/shard_map/all_to_all | solution.py:15
  28.6 6.7 %copy-start.17 = (f32[2,28,2]{1,2,0:T(2,128)S(1)}, f32[2,28,2]{1,2,0:T(2,128)}, u32[]{:S(2)}) copy-start(f32[2,28,2]{1,2,0:T(2,128)} %param.25) | copy-start | bytes 1348
  28.6 7.3 %copy-start.20 = (f32[2,2]{1,0:T(2,128)S(1)}, f32[2,2]{1,0:T(2,128)}, u32[]{:S(2)}) copy-start(f32[2,2]{1,0:T(2,128)} %param.20) | copy-start | bytes 52
  28.6 7.9 %copy-start.18 = (f32[2,2,128]{2,1,0:T(2,128)S(1)}, f32[2,2,128]{2,1,0:T(2,128)}, u32[]{:S(2)}) copy-start(f32[2,2,128]{2,1,0:T(2,128)} %param.21) | copy-start | bytes 6148
  29.3 21.7 %copy-start.5 = (f32[2,28,2,128]{3,2,1,0:T(2,128)S(1)}, f32[2,28,2,128]{3,2,1,0:T(2,128)}, u32[]{:S(2)}) copy-start(f32[2,28,2,128]{3,2,1,0:T(2,128)} %param.24) | copy-start | bytes 172036
  30.5 20.1 %all-to-all-start.1 = ((f32[8,28,1028]{2,1,0:T(8,128)}), f32[8,28,1028]{2,1,0:T(8,128)S(1)}, u32[]{:S(2)}, u32[]{:S(2)}) async-start(f32[8,28,1028]{2,1,0:T(8,128)} %reshape.187), calls=%async_computation.1 | async-start | bytes 2359296 | tf_op jit(solution)/shard_map/all_to_all | solution.py:32
  35.3 31.2 %copy-start = (bf16[2,256,512]{2,1,0:T(8,128)(2,1)S(1)}, bf16[2,256,512]{2,1,0:T(8,128)(2,1)}, u32[]{:S(2)}) copy-start(bf16[2,256,512]{2,1,0:T(8,128)(2,1)} %param.22) | copy-start | bytes 1572868
  51.0 0.6 copy-start.6
  51.0 6.4 %copy-start.10 = (f32[28,2,128]{2,1,0:T(2,128)}, f32[28,2,128]{2,1,0:T(2,128)S(1)}, u32[]{:S(2)}) copy-start(f32[28,2,128]{2,1,0:T(2,128)S(1)} %mul.321) | copy-start | bytes 86020
  51.3 5.9 %copy-start.8 = (f32[28,2,128]{2,1,0:T(2,128)}, f32[28,2,128]{2,1,0:T(2,128)S(1)}, u32[]{:S(2)}) copy-start(f32[28,2,128]{2,1,0:T(2,128)S(1)} %get-tuple-element.13) | copy-start | bytes 86020
  51.6 38.9 %copy-start.1 = (bf16[2,512,256]{2,1,0:T(8,128)(2,1)S(1)}, bf16[2,512,256]{2,1,0:T(8,128)(2,1)}, u32[]{:S(2)}) copy-start(bf16[2,512,256]{2,1,0:T(8,128)(2,1)} %param.17) | copy-start | bytes 1572868
  57.2 33.5 %copy-start.2 = (bf16[2,512,256]{2,1,0:T(8,128)(2,1)S(1)}, bf16[2,512,256]{2,1,0:T(8,128)(2,1)}, u32[]{:S(2)}) copy-start(bf16[2,512,256]{2,1,0:T(8,128)(2,1)} %param.16) | copy-start | bytes 1572868
  57.2 33.8 %copy-start.3 = (bf16[2,512,256]{2,1,0:T(8,128)(2,1)S(1)}, bf16[2,512,256]{2,1,0:T(8,128)(2,1)}, u32[]{:S(2)}) copy-start(bf16[2,512,256]{2,1,0:T(8,128)(2,1)} %param.15) | copy-start | bytes 1572868
  92.3 11.0 %all-to-all-start.7 = ((f32[8,1,224]{2,1,0:T(1,128)}), f32[8,1,224]{2,1,0:T(1,128)S(1)}, u32[]{:S(2)}, u32[]{:S(2)}) async-start(f32[8,1,224]{2,1,0:T(1,128)} %broadcast_in_dim.22), calls=%async_computation.7 | async-start | bytes 16384 | tf_op jit(solution)/shard_map/all_to_all | solution.py:15
  99.7 8.8 %copy-start.16 = (f32[28,2]{0,1:T(2,128)S(1)}, f32[28,2]{0,1:T(2,128)}, u32[]{:S(2)}) copy-start(f32[28,2]{0,1:T(2,128)} %get-tuple-element.34) | copy-start | bytes 676
  101.5 22.4 %copy-start.19 = (f32[2]{0:T(128)S(1)}, f32[2]{0:T(128)}, u32[]{:S(2)}) copy-start(f32[2]{0:T(128)} %get-tuple-element.36) | copy-start | bytes 28
  101.8 24.7 %copy-start.9 = (f32[28,2,128]{2,1,0:T(2,128)S(1)}, f32[28,2,128]{2,1,0:T(2,128)}, u32[]{:S(2)}) copy-start(f32[28,2,128]{2,1,0:T(2,128)} %copy-done.8) | copy-start | bytes 86020
  101.8 24.7 %copy-start.11 = (f32[28,2,128]{2,1,0:T(2,128)S(1)}, f32[28,2,128]{2,1,0:T(2,128)}, u32[]{:S(2)}) copy-start(f32[28,2,128]{2,1,0:T(2,128)} %copy-done.10) | copy-start | bytes 86020
  103.3 20.6 %all-to-all-start.6 = ((f32[8,28,1028]{2,1,0:T(8,128)}), f32[8,28,1028]{2,1,0:T(8,128)S(1)}, u32[]{:S(2)}, u32[]{:S(2)}) async-start(f32[8,28,1028]{2,1,0:T(8,128)} %reshape.190), calls=%async_computation.6 | async-start | bytes 2359296 | tf_op jit(solution)/shard_map/all_to_all | solution.py:32
  124.9 9.1 %slice-start = ((s8[7340032]{0:T(1024)(128)(4,1)}), s8[3145728]{0:T(1024)(128)(4,1)S(1)}, s32[]{:S(2)}) async-start(s8[7340032]{0:T(1024)(128)(4,1)} %bitcast.115), calls=%async_computation.10 | async-start | bytes 6291456
  126.5 7.6 %slice-start.1 = ((s8[7340032]{0:T(1024)(128)(4,1)}), s8[4194304]{0:T(1024)(128)(4,1)S(1)}, s32[]{:S(2)}) async-start(s8[7340032]{0:T(1024)(128)(4,1)} %bitcast.115), calls=%async_computation.11 | async-start | bytes 8388608
  126.5 7.6 %copy-start.15 = (f32[28,2,128,1]{2,1,0,3:T(2,128)S(1)}, f32[28,2,128,1]{2,1,0,3:T(2,128)}, u32[]{:S(2)}) copy-start(f32[28,2,128,1]{2,1,0,3:T(2,128)} %reshape.199) | copy-start | bytes 86020
  134.0 4.0 %copy-start.12 = (f32[28,2,128]{2,1,0:T(2,128)S(1)}, f32[28,2,128]{2,1,0:T(2,128)}, u32[]{:S(2)}) copy-start(f32[28,2,128]{2,1,0:T(2,128)} %div.59) | copy-start | bytes 86020
  134.0 10.2 %copy-start.7 = (f32[28,2]{1,0:T(8,128)S(1)}, f32[28,2]{1,0:T(8,128)}, u32[]{:S(2)}) copy-start(f32[28,2]{1,0:T(8,128)} %copy-done.6) | copy-start | bytes 676
  134.0 10.2 %copy-start.13 = (f32[1,28,2,128]{3,2,1,0:T(2,128)S(1)}, f32[1,28,2,128]{3,2,1,0:T(2,128)}, u32[]{:S(2)}) copy-start(f32[1,28,2,128]{3,2,1,0:T(2,128)} %reshape.194) | copy-start | bytes 86020
  134.1 10.2 %copy-start.14 = (f32[1,28,2,128]{3,2,1,0:T(2,128)S(1)}, f32[1,28,2,128]{3,2,1,0:T(2,128)}, u32[]{:S(2)}) copy-start(f32[1,28,2,128]{3,2,1,0:T(2,128)} %reshape.195) | copy-start | bytes 86020
  138.9 9.5 %all-to-all-start.8 = ((bf16[8,28,256]{2,1,0:T(8,128)(2,1)}), bf16[8,28,256]{2,1,0:T(8,128)(2,1)S(1)}, u32[]{:S(2)}, u32[]{:S(2)}) async-start(bf16[8,28,256]{2,1,0:T(8,128)(2,1)} %broadcast_in_dim.23), calls=%async_computation.8 | async-start | bytes 262144 | tf_op jit(solution)/shard_map/all_to_all | solution.py:15
  150.4 11.4 %all-to-all-start.9 = ((bf16[16,14,512]{2,1,0:T(8,128)(2,1)}), bf16[16,14,512]{2,1,0:T(8,128)(2,1)S(1)}, u32[]{:S(2)}, u32[]{:S(2)}) async-start(bf16[16,14,512]{2,1,0:T(8,128)(2,1)} %reshape.193), calls=%async_computation.9 | async-start | bytes 524288 | tf_op jit(solution)/shard_map/all_to_all | solution.py:58
where the time goes:
time: 166 us; the launch traced here: 162 us
  starting transfers between devices  40.5 us (24%)
  waiting for transfers between devices  36.9 us (22%)
  blocking collectives  32.3 us (19%)
  other arithmetic  19.4 us (12%)
  matrix products  17.3 us (10%)
  local copies, waits for them, and re-layouts  14.8 us (9%)
    all_to_all x2, waiting for transfers between devices, sum_at_owner(): tiles = lax.all_to_all(in_blocks(value, dim, count), axis, 0, 0, tiled=True)  28.3 us
    all_to_all x4, starting transfers between devices, from_everyone(): lax.all_to_all(jnp.broadcast_to(value[None], (count, *value.shape)), axis...  26.9 us
    all_to_all x2, blocking collectives, from_everyone(): lax.all_to_all(jnp.broadcast_to(value[None], (count, *value.shape)), axis...  19.1 us
    all_to_all x1, blocking collectives, sum_at_owner(): tiles = lax.all_to_all(in_blocks(value, dim, count), axis, 0, 0, tiled=True)  13.1 us
    all_to_all x2, starting transfers between devices, sum_at_owner(): tiles = lax.all_to_all(in_blocks(value, dim, count), axis, 0, 0, tiled=True)  10 us
    dot_general x2, matrix products, cell_update(): jnp.einsum('bhd,bhde->bhe', queries, matrix_new, precision=lax.Precision....  9.18 us
    all_to_all x4, waiting for transfers between devices, from_everyone(): lax.all_to_all(jnp.broadcast_to(value[None], (count, *value.shape)), axis...  7.83 us
    add x1, other arithmetic, cell_update(): decays[..., None, None] * matrix  7.52 us
  transfers between devices with their start and end apart: 7, of which 6 were waited for; matrix products, arithmetic and copies ran while one was open for 14% of the time, Pallas kernels for 0%

commit v1 on v0

v1 whole, which is shorter than its diff:
```python
import functools

import jax
import jax.numpy as jnp
from jax import lax
from jax.experimental import pallas as pl
from jax.experimental.pallas import tpu as pltpu
from jax.sharding import PartitionSpec as P

HEAD = 128
CELLS = 2
norm_eps = 1e-06
head_eps = 1e-05
MESH = pl.DeviceIdType.MESH
F32 = jnp.float32
BF16 = jnp.bfloat16
ORDER = (2, 1, 3, 0)
OTHERS = (2, 1, 3)


def remote(src, dst, send, recv, tp, dp):
    return pltpu.make_async_remote_copy(
        src_ref=src,
        dst_ref=dst,
        send_sem=send,
        recv_sem=recv,
        device_id={"tp": tp, "dp": dp},
        device_id_type=MESH,
    )


NH = 2
RB = 16 // NH
V = 14 // NH
R2 = 2 * RB
GROUPS = (
    (("q",), ("k",), ("v", "o")),
    (("q",), ("k",), ("v", "o")),
)
EXACT = ({"q", "k", "v", "o"}, {"q"})
WIDE = (F32, BF16)
WROWS = (V, RB)
WNAMES = ("q", "k", "v", "o", "i", "f", "p")


def group_type(cell, group):
    return F32 if group[0] in EXACT[cell] else BF16


def group_shape(cell, group):
    rows = V if group_type(cell, group) == F32 and group[0] != "q" else RB
    return (NH, 4, len(group), 2, rows, 256)


def kernel(*refs):
    (tok, wq, wk, wv, wo, wi, wf, bias, gain, wp, mem, nrm, mxs) = refs[:13]
    res_out, mb, nb, mxb = refs[13:17]
    rest = list(refs[17:])
    take = lambda n: [rest.pop(0) for _ in range(n)]
    (tokb, biasb, gainb, xo, xb, wb, gb, wpb, gsel, hb, mh, ml,
     npad, mxt, mxpad, dec_s, kt_s, v_s, q_s, rd_s, pad_s) = take(21)
    ob, orb = take(2), take(2)
    ps, rs = [], []
    for cell in range(CELLS):
        ps.append(take(len(GROUPS[cell])))
        rs.append(take(len(GROUPS[cell])))
    (ag_s, ag_r, rs_s, rs_r, h_s, h_r, o_s, o_r, wl, ws, wr, m_i, s_i, t_i) = take(14)

    t = lax.axis_index("tp")
    d = lax.axis_index("dp")
    z, x = t // 4, t % 4
    y, c = d // 2, d % 2
    other = 2 * y + (1 - c)
    cs = x // 2
    mine = 2 * z + x % 2

    def own_weight(cell, i):
        if i < 4:
            return (wq, wk, wv, wo)[i].at[cell], wb.at[cell, c, i]
        if i < 6:
            return (wi, wf)[i - 4].at[cell], gb.at[cell, c, i - 4]
        return wp.at[cell], wpb.at[cell, c]

    def local_weight(cell, i):
        src, dst = own_weight(cell, i)
        return pltpu.make_async_copy(src, dst, wl.at[cell, i])

    def pair_weight(cell, i):
        src, dst = own_weight(cell, i)
        return remote(src, dst, ws.at[cell, i], wr.at[cell, i], t, other)

    def have_weight(cell, i):
        local_weight(cell, i).wait()
        pair_weight(cell, i).wait_recv()

    def states_in(cell):
        return (
            pltpu.make_async_copy(nrm.at[cell], nb.at[cell], s_i.at[cell, 0]),
            pltpu.make_async_copy(mxs.at[cell], mxb.at[cell], s_i.at[cell, 1]),
            pltpu.make_async_copy(mem.at[cell], mb.at[cell], m_i.at[cell]),
        )

    small = (
        pltpu.make_async_copy(tok, tokb, t_i.at[0]),
        pltpu.make_async_copy(bias, biasb, t_i.at[1]),
        pltpu.make_async_copy(gain, gainb, t_i.at[2]),
    )
    for cp in small:
        cp.start()

    barrier = pltpu.get_barrier_semaphore()

    def greet(tp, dp):
        pl.semaphore_signal(barrier, inc=1, device_id={"tp": tp, "dp": dp}, device_id_type=MESH)

    for dz in ORDER:
        for dx in ORDER:
            t2 = ((z + dz) % 4) * 4 + (x + dx) % 4
            if dz == 0 and dx == 0:
                greet(t, other)
            else:
                greet(t2, 2 * y)
                greet(t2, 2 * y + 1)
    for dy in (2, 1, 3):
        greet(t, 2 * ((y + dy) % 4) + c)

    for i in (4, 5, 0, 1, 2, 3, 6):
        local_weight(0, i).start()
    for cp in states_in(0):
        cp.start()

    xo[...] = jnp.zeros_like(xo)
    npad[...] = jnp.zeros_like(npad)
    mxt[...] = jnp.zeros_like(mxt)
    rd_s[...] = jnp.zeros_like(rd_s)
    pad_s[...] = jnp.zeros_like(pad_s)
    for cp in small:
        cp.wait()
    for hf in range(NH):
        xo[0, hf, 0:V, :] = tokb[V * hf:V * hf + V, :]

    pl.semaphore_wait(barrier, 34)

    def gather(cell, hf):
        out = []
        k = 0
        for dz in ORDER:
            for dx in ORDER:
                t2 = ((z + dz) % 4) * 4 + (x + dx) % 4
                cp = remote(
                    xo.at[cell, hf], xb.at[cell, hf, c, mine], ag_s.at[cell, hf, k], ag_r.at[cell, hf, c, mine],
                    t2, 2 * y + cs,
                )
                out.append((cp, cs != c if dz == 0 and dx == 0 else None))
                k += 1
        return out

    def gather_in(cell, hf):
        out = []
        for c2 in range(2):
            for j in range(8):
                t2 = 4 * (j // 2) + 2 * c + j % 2
                cp = remote(
                    xo.at[cell, hf], xb.at[cell, hf, c2, j], ag_s.at[cell, hf, 0], ag_r.at[cell, hf, c2, j],
                    t2, 2 * y + c2,
                )
                out.append((cp, jnp.logical_or(t2 != t, c2 != c)))
        return out

    def spread(cell, hf, k):
        out = []
        for b in range(2):
            x2 = 2 * c + b
            for c2 in range(2):
                cp = remote(
                    ob[cell].at[hf, c2, 2 * k + b], orb[cell].at[hf, t],
                    o_s.at[cell, hf, 4 * k + 2 * b + c2], o_r.at[cell, hf, t], 4 * k + x2, 2 * y + c2,
                )
                out.append((cp, jnp.logical_or(jnp.logical_or(k != z, x2 != x), c2 != c)))
        return out

    def spread_in(cell, hf):
        out = []
        for t2 in range(16):
            cp = remote(
                ob[cell].at[hf, 0, 0], orb[cell].at[hf, t2], o_s.at[cell, hf, 0], o_r.at[cell, hf, t2], t2, 2 * y + cs
            )
            out.append((cp, jnp.logical_or(t != t2, cs != c)))
        return out

    def across(cell, hf, n):
        src, dst = ps[cell][n], rs[cell][n]
        out = []
        for dy in (2, 1, 3):
            y2 = (y + dy) % 4
            out.append(remote(
                src.at[hf, y2], dst.at[hf, y], rs_s.at[cell, hf, n, dy], rs_r.at[cell, hf, n, y], t, 2 * y2 + c
            ))
        return out

    def across_in(cell, hf, n):
        src, dst = ps[cell][n], rs[cell][n]
        out = []
        for dy in (1, 3, 2):
            y2 = (y + dy) % 4
            out.append(remote(
                src.at[hf, y], dst.at[hf, y2], rs_s.at[cell, hf, n, dy], rs_r.at[cell, hf, n, y2], t, 2 * y2 + c
            ))
        return out

    def hid(cell, hf):
        return [
            remote(hb.at[cell, hf, y], hb.at[cell, hf, y], h_s.at[cell, hf, dy], h_r.at[cell, hf, y],
                   t, 2 * ((y + dy) % 4) + c)
            for dy in (2, 1, 3)
        ]

    def hid_in(cell, hf):
        out = []
        for dy in (1, 3, 2):
            y2 = (y + dy) % 4
            out.append(remote(
                hb.at[cell, hf, y], hb.at[cell, hf, y2], h_s.at[cell, hf, dy], h_r.at[cell, hf, y2], t, 2 * y2 + c
            ))
        return out

    def each(pairs, what):
        for cp, cond in pairs:
            if cond is None:
                getattr(cp, what)()
            else:
                @pl.when(cond)
                def _():
                    getattr(cp, what)()

    for hf in range(NH):
        each(gather(0, hf), "start")
    for i in (4, 5, 0, 1, 2, 3, 6):
        pair_weight(0, i).start()
    for cp in states_in(1):
        cp.start()
    for i in range(7):
        local_weight(1, i).start()
    for i in range(7):
        pair_weight(1, i).start()

    row = lax.broadcasted_iota(jnp.int32, (R2, HEAD), 0)
    pad_row = lax.broadcasted_iota(jnp.int32, (R2, 256), 0) == V
    gate_row = lax.broadcasted_iota(jnp.int32, (HEAD, 512), 0)
    ones_at = jnp.where(gate_row // R2 == 4, 1.0, 0.0).astype(BF16)
    own_lane = lax.broadcasted_iota(jnp.int32, (R2, HEAD), 1) % R2 == row

    def nt(a, b):
        return lax.dot_general(a, b, (((1,), (1,)), ((), ())), preferred_element_type=F32)

    def prepare(cell):
        have_weight(cell, 4)
        have_weight(cell, 5)
        for g in range(2):
            want = lax.broadcasted_iota(jnp.int32, (HEAD, 32), 0) // R2 - 2 * g
            head = lax.broadcasted_iota(jnp.int32, (HEAD, 32), 1)
            pick = jnp.logical_and(jnp.logical_and(want >= 0, want < 2), head == 2 * t + want)
            pick = jnp.where(pick, 1.0, 0.0).astype(BF16)
            for c2 in range(2):
                part = jnp.dot(pick, gb[cell, c2, g], preferred_element_type=F32).astype(BF16)
                if g == 0:
                    gsel[cell, c2] = part
                else:
                    gsel[cell, c2] = gsel[cell, c2] + part
        cps = states_in(cell)
        for cp in cps:
            cp.wait()
        for hf in range(NH):
            for s in range(2):
                at = 14 * s + V * hf
                mxt[cell, hf, 0:2, RB * s:RB * s + V] = mxb[cell, :, at:at + V]
                for h in range(2):
                    npad[cell, hf, h, RB * s:RB * s + V, :] = nb[cell, pl.ds(2 * at + h, V, stride=2), :]
            mxpad[cell, hf] = mxt[cell, hf].T

        def split(b, carry):
            for h in range(2):
                m = mb[cell, b, h]
                high = m.astype(BF16)
                mh[cell, b, h] = high
                if cell == 0:
                    ml[b, h] = (m - high.astype(F32)).astype(BF16)
            return carry

        lax.fori_loop(0, 28, split, 0, unroll=2)

    def project(cell, parts):
        for hf in parts:
            @pl.when(cs == c)
            def _():
                xb[cell, hf, c, mine] = xo[cell, hf]

        for hf in parts:
            each(gather_in(cell, hf), "wait_recv")
        x0, x1 = (
            jnp.concatenate([xb[cell, hf, c2].reshape(8 * RB, 512) for hf in parts], axis=0) for c2 in range(2)
        )
        gates = nt(x0, gsel[cell, 0]) + nt(x1, gsel[cell, 1]) + nt(x0 * x0, ones_at) + nt(x1 * x1, ones_at)
        gates = gates.reshape(len(parts), 4, R2, HEAD)
        gates = jnp.sum(jnp.where(own_lane[None, None], gates, 0.0), axis=2, keepdims=True)
        for n, group in enumerate(GROUPS[cell]):
            dst = ps[cell][n]
            for m, name in enumerate(group):
                i = WNAMES.index(name)
                if parts[0] == 0:
                    have_weight(cell, i)
                acc = jnp.dot(x0, wb[cell, 0, i], preferred_element_type=F32)
                acc += jnp.dot(x1, wb[cell, 1, i], preferred_element_type=F32)
                acc = acc.astype(dst.dtype).reshape(len(parts), 4, 2, RB, 256)
                for k, hf in enumerate(parts):
                    dst[hf, :, m] = acc[k, :, :, 0:dst.shape[4]]
                    if name == "q":
                        dst[hf, :, m, 0, V:V + 1, 0:HEAD] = gates[k]
            for hf in parts:
                for cp in across(cell, hf, n):
                    cp.start()

    def total(cell, hf, name):
        for n, group in enumerate(GROUPS[cell]):
            if name not in group:
                continue
            if name == group[0]:
                for cp in across_in(cell, hf, n):
                    cp.wait_recv()
            m = group.index(name)
            ref = rs[cell][n]
            mine_ref = ps[cell][n]
            out = mine_ref[hf, y, m].astype(F32)
            for dy in (1, 2, 3):
                out = out + ref[hf, (y + dy) % 4, m].astype(F32)
            if out.shape[1] == RB:
                return out.reshape(R2, 256)
            for s in range(2):
                pad_s[cell, hf, WNAMES.index(name) - 1, RB * s:RB * s + V] = out[s]
            return pad_s[cell, hf, WNAMES.index(name) - 1]

    def heads(cell, hf):
        queries = total(cell, hf, "q")
        flat = jnp.where(own_lane, jnp.broadcast_to(queries[V:V + 1, 0:HEAD], (R2, HEAD)), 0.0)
        which = lax.broadcasted_iota(jnp.int32, (R2, HEAD), 1) // R2
        gate = [jnp.sum(jnp.where(which == k, flat, 0.0), axis=1, keepdims=True) for k in range(5)]
        queries = jnp.where(pad_row, 0.0, queries)
        inv = lax.rsqrt(gate[4] / 4096 + norm_eps)
        decs, wins = [], []
        for h in range(2):
            log_in = gate[h] * inv
            f = gate[2 + h] * inv + biasb[cell, h]
            log_forget = jnp.minimum(f, 0.0) - jnp.log1p(jnp.exp(-jnp.abs(f)))
            old = log_forget + mxpad[cell, hf, 0:R2, h:h + 1]
            new = jnp.maximum(old, log_in)
            mxpad[cell, hf, 0:R2, h:h + 1] = new
            decs.append(jnp.exp(old - new))
            wins.append(jnp.exp(log_in - new))
            dec_s[cell, hf, h] = jnp.broadcast_to(decs[h], (R2, HEAD))
        queries = queries * inv
        keys = total(cell, hf, "k") * inv * HEAD ** (-0.5)
        alphas, dens = [], []
        for h in range(2):
            qh = queries[:, HEAD * h:HEAD * (h + 1)]
            q_s[h] = qh
            wkey = keys[:, HEAD * h:HEAD * (h + 1)] * wins[h]
            kt_s[cell, hf, h] = wkey.T.astype(BF16)
            new = decs[h] * npad[cell, hf, h] + wkey
            npad[cell, hf, h] = new
            alphas.append(jnp.sum(qh * wkey, axis=-1, keepdims=True))
            dens.append(jnp.maximum(jnp.abs(jnp.sum(qh * new, axis=-1, keepdims=True)), 1.0))

        for s in range(2):
            for i in range(V):
                r = RB * s + i
                b = 14 * s + V * hf + i
                for h in range(2):
                    q_row = jnp.broadcast_to(q_s[h, r:r + 1, :], (8, HEAD))
                    q_high = q_row.astype(BF16).astype(F32)
                    both = jnp.concatenate([q_high, q_row - q_high], axis=0).astype(BF16)
                    read = jnp.dot(both, mh[cell, b, h], preferred_element_type=F32)
                    if cell == 0:
                        read = read[0:8] + read[8:16] + jnp.dot(both, ml[b, h], preferred_element_type=F32)[0:8]
                    rd_s[h, r:r + 1, :] = read[0:1]

        values = total(cell, hf, "v") * inv
        outgate = total(cell, hf, "o") * inv
        for h in range(2):
            value = values[:, HEAD * h:HEAD * (h + 1)]
            v_s[cell, hf, h] = value
            read = (decs[h] * rd_s[h] + alphas[h] * value) / dens[h]
            mean = jnp.mean(read, axis=-1, keepdims=True)
            var = jnp.mean(jnp.square(read - mean), axis=-1, keepdims=True)
            normed = (read - mean) * lax.rsqrt(var + head_eps) * gainb[cell, h:h + 1, :]
            hidden = normed * jax.nn.sigmoid(outgate[:, HEAD * h:HEAD * (h + 1)])
            hb[cell, hf, y, :, HEAD * h:HEAD * (h + 1)] = hidden.astype(BF16)
        for cp in hid(cell, hf):
            cp.start()
        if hf == 0:
            have_weight(cell, 6)
        out_pieces(cell, hf, (0,))
        each(spread(cell, hf, y), "start")

    def out_pieces(cell, hf, dys):
        ks = [(y + dy) % 4 for dy in dys]
        hid_rows = jnp.concatenate([hb[cell, hf, k] for k in ks], axis=0)
        for c2 in range(2):
            acc = jnp.dot(hid_rows, wpb[cell, c2], preferred_element_type=F32)
            acc = acc.astype(WIDE[cell]).reshape(len(dys), 2, RB, 512)[:, :, 0:WROWS[cell]]
            for at, k in enumerate(ks):
                ob[cell][hf, c2, pl.ds(2 * k, 2)] = acc[at]

    def outputs(cell, hf):
        for cp in hid_in(cell, hf):
            cp.wait_recv()
        out_pieces(cell, hf, OTHERS)
        for dz in ORDER:
            z2 = (z + dz) % 4
            for cp, cond in spread(cell, hf, z2):
                @pl.when(jnp.logical_and(z2 != y, cond))
                def _():
                    cp.start()

        @pl.when(cs == c)
        def _():
            orb[cell][hf, t] = ob[cell][hf, c, mine]

    def update(cell):
        for hf in range(NH):
            mxt[cell, hf] = mxpad[cell, hf].T
            for s in range(2):
                at = 14 * s + V * hf
                mxb[cell, :, at:at + V] = mxt[cell, hf, 0:2, RB * s:RB * s + V]
                for h in range(2):
                    nb[cell, pl.ds(2 * at + h, V, stride=2), :] = npad[cell, hf, h, RB * s:RB * s + V, :]

            def one(i, carry):
                for s in range(2):
                    r = RB * s + i
                    b = 14 * s + V * hf + i
                    for h in range(2):
                        v_row = jnp.where(row == r, v_s[cell, hf, h], 0.0).astype(BF16)
                        outer = jnp.dot(kt_s[cell, hf, h], v_row, preferred_element_type=F32)
                        mb[cell, b, h] = dec_s[cell, hf, h, pl.ds(r, 1), :] * mb[cell, b, h] + outer
                return carry

            lax.fori_loop(0, V, one, 0)

    def collect(cell, hf):
        each(spread_in(cell, hf), "wait_recv")
        tot = orb[cell][hf, 0].astype(F32)
        for t2 in range(1, 16):
            tot += orb[cell][hf, t2].astype(F32)
        xo[cell + 1, hf, 0:WROWS[cell]] = tot.astype(BF16)
        if cell + 1 < CELLS:
            each(gather(cell + 1, hf), "start")

    def settle(cell):
        for hf in range(NH):
            each(gather(cell, hf), "wait_send")
            if cell:
                for k in range(4):
                    each(spread(cell - 1, hf, k), "wait_send")
            for n in range(len(GROUPS[cell])):
                for cp in across(cell, hf, n):
                    cp.wait_send()
            for cp in hid(cell, hf):
                cp.wait_send()
        for i in range(7):
            pair_weight(cell, i).wait_send()

    prepare(0)
    for cell in range(CELLS):
        for parts in [(hf,) for hf in range(NH)]:
            project(cell, parts)
        for hf in range(NH):
            heads(cell, hf)
        for hf in range(NH):
            outputs(cell, hf)
        update(cell)
        if cell + 1 < CELLS:
            prepare(cell + 1)
        settle(cell)
        for hf in range(NH):
            collect(cell, hf)
    for hf in range(NH):
        res_out[V * hf:V * hf + V, :] = xo[CELLS, hf, 0:V, :]

    for hf in range(NH):
        for k in range(4):
            each(spread(CELLS - 1, hf, k), "wait_send")


def flush(res, mb, nb, mxb, res_out, mem_out, nrm_out, mxs_out, sems):
    cps = [
        pltpu.make_async_copy(
            mb.at[i // 4, pl.ds(7 * (i % 4), 7)], mem_out.at[i // 4, pl.ds(7 * (i % 4), 7)], sems.at[i]
        )
        for i in range(8)
    ]
    cps.append(pltpu.make_async_copy(res, res_out, sems.at[8]))
    cps.append(pltpu.make_async_copy(nb, nrm_out, sems.at[9]))
    cps.append(pltpu.make_async_copy(mxb, mxs_out, sems.at[10]))
    for cp in cps:
        cp.start()
    for cp in cps:
        cp.wait()


def on_device(tokens, wq, wk, wv, wo, wi, wf, bias, gain, wp, mem, nrm, mxs):
    hbm = pl.BlockSpec(memory_space=pltpu.HBM)
    vmem = pl.BlockSpec(memory_space=pltpu.VMEM)
    dma = pltpu.SemaphoreType.DMA
    nrm2 = nrm.reshape(CELLS, 56, HEAD)
    mxs2 = mxs.transpose(0, 2, 1)
    wi2 = wi.transpose(0, 2, 1)
    wf2 = wf.transpose(0, 2, 1)
    shapes = (
        jax.ShapeDtypeStruct((14, 512), BF16),
        jax.ShapeDtypeStruct(mem.shape, F32),
        jax.ShapeDtypeStruct(nrm2.shape, F32),
        jax.ShapeDtypeStruct(mxs2.shape, F32),
    )
    held = pl.pallas_call(
        kernel,
        out_shape=tuple(pltpu.VMEM(a.shape, a.dtype) for a in shapes),
        in_specs=[hbm] * 13,
        out_specs=(vmem,) * 4,
        scratch_shapes=[
            pltpu.VMEM((14, 512), BF16),
            pltpu.SMEM((CELLS, 2), F32),
            pltpu.VMEM((CELLS, 2, HEAD), F32),
            pltpu.VMEM((CELLS + 1, NH, RB, 512), BF16),
            pltpu.VMEM((CELLS, NH, 2, 8, RB, 512), BF16),
            pltpu.VMEM((CELLS, 2, 4, 512, 256), BF16),
            pltpu.VMEM((CELLS, 2, 2, 32, 512), BF16),
            pltpu.VMEM((CELLS, 2, 256, 512), BF16),
            pltpu.VMEM((CELLS, 2, HEAD, 512), BF16),
            pltpu.VMEM((CELLS, NH, 4, R2, 256), BF16),
            pltpu.VMEM((CELLS, 28, 2, HEAD, HEAD), BF16),
            pltpu.VMEM((28, 2, HEAD, HEAD), BF16),
            pltpu.VMEM((CELLS, NH, 2, R2, HEAD), F32),
            pltpu.VMEM((CELLS, NH, 8, HEAD), F32),
            pltpu.VMEM((CELLS, NH, HEAD, 8), F32),
            pltpu.VMEM((CELLS, NH, 2, R2, HEAD), F32),
            pltpu.VMEM((CELLS, NH, 2, HEAD, R2), BF16),
            pltpu.VMEM((CELLS, NH, 2, R2, HEAD), F32),
            pltpu.VMEM((2, R2, HEAD), F32),
            pltpu.VMEM((2, R2, HEAD), F32),
            pltpu.VMEM((1, NH, 3, R2, 256), F32),
            *(pltpu.VMEM((NH, 2, 8, WROWS[cell], 512), WIDE[cell]) for cell in range(CELLS)),
            *(pltpu.VMEM((NH, 16, WROWS[cell], 512), WIDE[cell]) for cell in range(CELLS)),
            *(
                pltpu.VMEM(group_shape(cell, group), group_type(cell, group))
                for cell in range(CELLS) for _ in range(2) for group in GROUPS[cell]
            ),
            dma((CELLS, NH, 16)), dma((CELLS, NH, 2, 8)),
            dma((CELLS, NH, 4, 4)), dma((CELLS, NH, 4, 4)),
            dma((CELLS, NH, 4)), dma((CELLS, NH, 4)),
            dma((CELLS, NH, 16)), dma((CELLS, NH, 16)),
            dma((CELLS, 7)), dma((CELLS, 7)), dma((CELLS, 7)),
            dma((CELLS,)), dma((CELLS, 2)), dma((3,)),
        ],
        compiler_params=pltpu.CompilerParams(
            collective_id=0, has_side_effects=True, vmem_limit_bytes=48 * 1024 * 1024
        ),
    )(*(pltpu.with_memory_space_constraint(a, pltpu.HBM) for a in (tokens, wq, wk, wv, wo, wi2, wf2, bias, gain, wp, mem, nrm2, mxs2)))
    res, mem_new, nrm_new, mxs_new = pl.pallas_call(
        flush,
        out_shape=shapes,
        in_specs=[vmem] * 4,
        out_specs=(hbm,) * 4,
        scratch_shapes=[dma((11,))],
        compiler_params=pltpu.CompilerParams(vmem_limit_bytes=1024 * 1024),
    )(*held)
    return res, mem_new, nrm_new.reshape(nrm.shape), mxs_new.transpose(0, 2, 1)


def solution(mesh):
    in_specs = (
        P("tp", "dp"),
        P(None, "dp", "tp"),
        P(None, "dp", "tp"),
        P(None, "dp", "tp"),
        P(None, "dp", "tp"),
        P(None, "dp", None),
        P(None, "dp", None),
        P(None, "tp"),
        P(None, "tp", None),
        P(None, "tp", "dp"),
        P(None, "dp", "tp", None, None),
        P(None, "dp", "tp", None),
        P(None, "dp", "tp"),
    )
    out_specs = (
        P("tp", "dp"),
        P(None, "dp", "tp", None, None),
        P(None, "dp", "tp", None),
        P(None, "dp", "tp"),
    )
    return jax.shard_map(on_device, mesh=mesh, in_specs=in_specs, out_specs=out_specs, check_vma=False)
```

time: 166 us -> 59 us (0.36); the launches traced: 162 us -> 58.9 us
  Pallas kernels: 0 us -> 58.2 us
  starting transfers between devices: 40.5 us -> 0 us
  waiting for transfers between devices: 36.9 us -> 0 us
  blocking collectives: 32.3 us -> 0 us
  other arithmetic: 19.4 us -> 0 us
  matrix products: 17.3 us -> 0 us
  local copies, waits for them, and re-layouts: 14.8 us -> 0 us
    pallas_call x0 -> x2, Pallas kernels: none -> 58.2 us  [the longest x1 55.1 us: on_device(): pl.pallas_call(kernel, out_shape=tuple((pltpu.VMEM(a.shape, a.dtype) for...]
    all_to_all x7 -> x0, starting transfers between devices: 40.5 us -> none  [the longest x4 26.9 us: from_everyone(): lax.all_to_all(jnp.broadcast_to(value[None], (count, *value.shape)), axis...]
    all_to_all x7 -> x0, waiting for transfers between devices: 36.9 us -> none  [the longest x2 28.3 us: sum_at_owner(): tiles = lax.all_to_all(in_blocks(value, dim, count), axis, 0, 0, tiled=True)]
    all_to_all x3 -> x0, blocking collectives: 32.3 us -> none  [the longest x2 19.1 us: from_everyone(): lax.all_to_all(jnp.broadcast_to(value[None], (count, *value.shape)), axis...]
    dot_general x16 -> x0, matrix products: 17.3 us -> none  [the longest x2 9.18 us: cell_update(): jnp.einsum('bhd,bhde->bhe', queries, matrix_new, precision=lax.Precision....]
    another operation x3 -> x0, other arithmetic: 8.39 us -> none  [the longest x1 7.16 us: on_device(): jnp.stack(matrix_list)]
    add x2 -> x0, other arithmetic: 7.71 us -> none  [the longest x1 7.52 us: cell_update(): decays[..., None, None] * matrix]
    reshape x12 -> x0, local copies, waits for them, and re-layouts: 5.09 us -> none  [the longest x3 2.99 us: in_blocks(): return jnp.moveaxis(value.reshape(*before, count, -1, *after), dim, 0)]
  transfers between devices with their start and end apart: 7 -> 0, of which waited for: 6 -> 0; matrix products, arithmetic and copies ran while one was open for 14% -> 0% of each run, Pallas kernels for 0% -> 0%
where the time goes in v1:
time: 59 us; the launch traced here: 58.9 us
  Pallas kernels  58.2 us (99%)
  between operations  0.64 us (1%)
    pallas_call x1, Pallas kernels, on_device(): pl.pallas_call(kernel, out_shape=tuple((pltpu.VMEM(a.shape, a.dtype) for...  55.1 us
    pallas_call x1, Pallas kernels, on_device(): pl.pallas_call(flush, out_shape=shapes, in_specs=[vmem] * 4, out_specs=(h...  3.09 us

profile of v1, /device:TPU:9, one launch (start us, length us, event | category | flops | bytes accessed | tf_op | source)
XLA Modules:
  0.0 58.9 jit_solution(18093604447770449996)
XLA Ops:
  0.6 55.1 %shard_map.156 = (bf16[14,512]{1,0:T(8,128)(2,1)S(1)}, f32[2,28,2,128,128]{4,3,2,1,0:T(8,128)S(1)}, f32[2,56,128]{2,1,0:T(8,128)S(1)}, f32[2,2,28]{2,1,0:T(2,128)S(1)}) custom-call(bf16[14,512]{1,0:T(8,128)(2,1)} %refs_0_.1, bf16[2,512,256]{2,1,0:T(8,128)(2,1)} %refs_1_.1, bf16[2,512,256]{2,1,0:T(8,128)(2,1)} %refs_2_.1, bf16[2,512,256]{2,1,0:T(8,128)(2,1)} %refs_3_.1, ...), custom_call_target="tpu_custom_call" | custom-call | tf_op jit(solution)/shard_map/pallas_call | solution.py:524
  55.8 3.1 %shard_map.157 = (bf16[14,512]{1,0:T(8,128)(2,1)}, f32[2,28,2,128,128]{4,3,2,1,0:T(8,128)}, f32[2,56,128]{2,1,0:T(8,128)}, f32[2,2,28]{2,1,0:T(2,128)}) custom-call(bf16[14,512]{1,0:T(8,128)(2,1)S(1)} %get-tuple-element.12.res, f32[2,28,2,128,128]{4,3,2,1,0:T(8,128)S(1)} %get-tuple-element.13.mb, f32[2,56,128]{2,1,0:T(8,128)S(1)} %get-tuple-element.14.nb, ...), custom_call_target="tpu_custom_call" | custom-call | tf_op jit(solution)/shard_map/pallas_call | solution.py:568

commit v2 on v1

--- a/solution.py
+++ b/solution.py
@@ -233,10 +233,11 @@
                 def _():
                     getattr(cp, what)()
 
-    for hf in range(NH):
-        each(gather(0, hf), "start")
+    each(gather(0, 0), "start")
     for i in (4, 5, 0, 1, 2, 3, 6):
         pair_weight(0, i).start()
+    for hf in range(1, NH):
+        each(gather(0, hf), "start")
     for cp in states_in(1):
         cp.start()
     for i in range(7):
@@ -358,18 +359,8 @@
             wins.append(jnp.exp(log_in - new))
             dec_s[cell, hf, h] = jnp.broadcast_to(decs[h], (R2, HEAD))
         queries = queries * inv
-        keys = total(cell, hf, "k") * inv * HEAD ** (-0.5)
-        alphas, dens = [], []
         for h in range(2):
-            qh = queries[:, HEAD * h:HEAD * (h + 1)]
-            q_s[h] = qh
-            wkey = keys[:, HEAD * h:HEAD * (h + 1)] * wins[h]
-            kt_s[cell, hf, h] = wkey.T.astype(BF16)
-            new = decs[h] * npad[cell, hf, h] + wkey
-            npad[cell, hf, h] = new
-            alphas.append(jnp.sum(qh * wkey, axis=-1, keepdims=True))
-            dens.append(jnp.maximum(jnp.abs(jnp.sum(qh * new, axis=-1, keepdims=True)), 1.0))
-
+            q_s[h] = queries[:, HEAD * h:HEAD * (h + 1)]
         for s in range(2):
             for i in range(V):
                 r = RB * s + i
@@ -382,6 +373,17 @@
                     if cell == 0:
                         read = read[0:8] + read[8:16] + jnp.dot(both, ml[b, h], preferred_element_type=F32)[0:8]
                     rd_s[h, r:r + 1, :] = read[0:1]
+
+        keys = total(cell, hf, "k") * inv * HEAD ** (-0.5)
+        alphas, dens = [], []
+        for h in range(2):
+            qh = queries[:, HEAD * h:HEAD * (h + 1)]
+            wkey = keys[:, HEAD * h:HEAD * (h + 1)] * wins[h]
+            kt_s[cell, hf, h] = wkey.T.astype(BF16)
+            new = decs[h] * npad[cell, hf, h] + wkey
+            npad[cell, hf, h] = new
+            alphas.append(jnp.sum(qh * wkey, axis=-1, keepdims=True))
+            dens.append(jnp.maximum(jnp.abs(jnp.sum(qh * new, axis=-1, keepdims=True)), 1.0))
 
         values = total(cell, hf, "v") * inv
         outgate = total(cell, hf, "o") * inv

time: 59 us -> 59.2 us (level)
  no operation moved by 1% of the time
where the time goes in v2:
time: 59.2 us; the launch traced here: 59 us
  Pallas kernels  58.4 us (99%)
  between operations  0.64 us (1%)
    pallas_call x1, Pallas kernels, on_device(): pl.pallas_call(kernel, out_shape=tuple((pltpu.VMEM(a.shape, a.dtype) for...  55.3 us
    pallas_call x1, Pallas kernels, on_device(): pl.pallas_call(flush, out_shape=shapes, in_specs=[vmem] * 4, out_specs=(h...  3.09 us

profile of v2, /device:TPU:9, one launch (start us, length us, event | category | flops | bytes accessed | tf_op | source)
XLA Modules:
  0.0 59.0 jit_solution(15042674674262783774)
XLA Ops:
  0.6 55.3 %shard_map.156 = (bf16[14,512]{1,0:T(8,128)(2,1)S(1)}, f32[2,28,2,128,128]{4,3,2,1,0:T(8,128)S(1)}, f32[2,56,128]{2,1,0:T(8,128)S(1)}, f32[2,2,28]{2,1,0:T(2,128)S(1)}) custom-call(bf16[14,512]{1,0:T(8,128)(2,1)} %refs_0_.1, bf16[2,512,256]{2,1,0:T(8,128)(2,1)} %refs_1_.1, bf16[2,512,256]{2,1,0:T(8,128)(2,1)} %refs_2_.1, bf16[2,512,256]{2,1,0:T(8,128)(2,1)} %refs_3_.1, ...), custom_call_target="tpu_custom_call" | custom-call | tf_op jit(solution)/shard_map/pallas_call | solution.py:526
  55.9 3.1 %shard_map.157 = (bf16[14,512]{1,0:T(8,128)(2,1)}, f32[2,28,2,128,128]{4,3,2,1,0:T(8,128)}, f32[2,56,128]{2,1,0:T(8,128)}, f32[2,2,28]{2,1,0:T(2,128)}) custom-call(bf16[14,512]{1,0:T(8,128)(2,1)S(1)} %get-tuple-element.12.res, f32[2,28,2,128,128]{4,3,2,1,0:T(8,128)S(1)} %get-tuple-element.13.mb, f32[2,56,128]{2,1,0:T(8,128)S(1)} %get-tuple-element.14.nb, ...), custom_call_target="tpu_custom_call" | custom-call | tf_op jit(solution)/shard_map/pallas_call | solution.py:570
